TPU v7x, 256 devices: a 4x2x16 block of a 4x16x16 slice. The times are simulated.
256 devices in a mesh: grp: 2 (over y), sp: 32 (over z, core), tp: 4 (over x).
Axes of the slice: x: 4, y: 2, z: 16, core: 2. Of those that a mesh axis runs over, the one named last changes fastest.
The devices are a block of a 4x16x16 slice.
Arguments:
- stream: bfloat16 [16384, 2048], P(('grp', 'sp'), 'tp'), parts along dimension 0, may hold values from -1.5 to 1.5
- layer_norm_gain: float32 [2, 2048], replicated, may hold values from 0.1 to 1.9
- convolution_in_weight: bfloat16 [2, 2048, 1536], P(None, 'sp', 'tp'), may hold values from -0.125 to 0.125
- gating_in_weight: bfloat16 [2, 2048, 1536], P(None, 'sp', 'tp'), may hold values from -0.125 to 0.125
- output_weight: bfloat16 [2, 1536, 2048], P(None, 'tp', 'sp'), may hold values from -0.15625 to 0.15625
- convolution_kernel_taps: float32 [2, 4, 1536], P(None, None, 'tp'), may hold values from -12 to 12
- recurrent_gate_blocks: bfloat16 [2, 2, 2, 12, 128, 128], P(None, None, None, 'tp'), may hold values from -0.5 to 0.5
- channel_decay_logit: float32 [2, 2, 1536], P(None, None, 'tp')
- position_decay_boost: float32 [2, 2, 16384], P(None, None, ('grp', 'sp')), parts along dimension 2, may hold values from -1.4 to 0, as said below
Outputs:
- new_stream: bfloat16 [16384, 2048], P(('grp', 'sp'), 'tp'), parts along dimension 0
There are 2 independent parts, one for each index of `grp`. A program takes and returns all parts, laid end to end along the dimension named above; an argument that names none is the same for every part. Nothing has to cross between parts.
Inputs may be any that keep to these rules, and one draw needn't show every extreme that they name: `position_decay_boost`: zero at all but a few positions.
All inputs are finite; a program needn't handle non-finite values.
Results may differ from a plain program's by a relative error of at most 0.025.
Values may be sent and summed in bfloat16 or wider, within the bound.
A program may use at most 128 MiB of HBM per device.

v0:
```python
import jax
import jax.numpy as jnp
from jax import lax
from jax.sharding import PartitionSpec as P

EPS = 1e-06
RECURRENT_WIDTH = 8.0


def in_order(blocks, dim):
    blocks = jnp.moveaxis(blocks, 0, dim)
    dims = blocks.shape
    return blocks.reshape(*dims[:dim], dims[dim] * dims[dim + 1], *dims[dim + 2 :])


def sent_to_all(array, axis):
    size = lax.axis_size(axis)
    return lax.all_to_all(
        jnp.broadcast_to(array[None], (size, *array.shape)), axis, 0, 0, tiled=True
    )


def gathered_copies(array, axis, dim):
    return in_order(sent_to_all(array, axis), dim)


def extended(cells, sides, width):
    for axis, dim in sides:
        count = lax.axis_size(axis)
        ends = count - 1
        head = lax.slice_in_dim(cells, 0, width, axis=dim)
        tail = lax.slice_in_dim(cells, cells.shape[dim] - width, cells.shape[dim], axis=dim)
        cells = jnp.concatenate(
            [
                lax.ppermute(tail, axis, [(i, (i + 1) % count) for i in range(ends)]),
                cells,
                lax.ppermute(head, axis, [((i + 1) % count, i) for i in range(ends)]),
            ],
            axis=dim,
        )
    return cells


def sent_together(arrays, axis, dim, along):
    widths = [a.shape[along] for a in arrays]
    both = jnp.concatenate(arrays, axis=along)
    result = lax.all_gather(both, axis, axis=dim, tiled=True)
    return tuple(jnp.split(result, [sum(widths[:k]) for k in range(1, len(widths))], axis=along))


def split_up(array, dim, size):
    dims = array.shape
    blocks = array.reshape(*dims[:dim], size, dims[dim] // size, *dims[dim + 1 :])
    return jnp.moveaxis(blocks, dim, 0)


def sum_at_owner(array, axis, dim):
    size = lax.axis_size(axis)
    blocks = lax.all_to_all(split_up(array, dim, size), axis, 0, 0, tiled=True)
    return jnp.sum(blocks.astype(jnp.float32), axis=0)


def rms_norm(values, gain_row):
    floats = values.astype(jnp.float32)
    inverse = lax.rsqrt(jnp.mean(floats * floats, axis=-1, keepdims=True) + EPS)
    return (floats * inverse * gain_row).astype(jnp.bfloat16)


def combine_pairs(earlier, latter):
    return (earlier[0] * latter[0], latter[0] * earlier[1] + latter[1])


def local(
    stream,
    layer_norm_gain,
    convolution_in_weight,
    gating_in_weight,
    output_weight,
    convolution_kernel_taps,
    recurrent_gate_blocks,
    channel_decay_logit,
    position_decay_boost,
):
    tok_rows = stream.shape[0]
    channels = convolution_in_weight.shape[2]
    gate_count = recurrent_gate_blocks.shape[3]
    block_width = recurrent_gate_blocks.shape[4]
    seq_devices = lax.axis_size("sp")
    my_index = lax.axis_index("sp")
    seq_length = tok_rows * seq_devices
    positions = my_index * tok_rows + lax.iota(jnp.int32, tok_rows)
    at_first = (positions == 0)[:, None]
    at_last = (positions == seq_length - 1)[:, None]
    all_x, all_y, all_out = (
        lax.all_gather(convolution_in_weight, "sp", axis=1, tiled=True),
        lax.all_gather(gating_in_weight, "sp", axis=1, tiled=True),
        lax.all_gather(output_weight, "sp", axis=2, tiled=True),
    )
    for layer_index in range(convolution_in_weight.shape[0]):
        features = gathered_copies(stream, "tp", 1)
        normed = rms_norm(features, layer_norm_gain[layer_index])
        proj_x = jnp.dot(normed, all_x[layer_index], preferred_element_type=jnp.float32).astype(
            jnp.bfloat16
        )
        proj_y = jnp.dot(normed, all_y[layer_index], preferred_element_type=jnp.float32).astype(
            jnp.bfloat16
        )
        padded = extended(proj_x, (("sp", 0),), 2).astype(jnp.float32)
        taps_now = convolution_kernel_taps[layer_index]
        conv_mixed = (
            taps_now[0] * padded[1 : tok_rows + 1]
            + taps_now[1] * padded[2 : tok_rows + 2]
            + taps_now[2] * padded[3 : tok_rows + 3]
            + taps_now[3] * padded[4 : tok_rows + 4]
        )
        convolution_output = conv_mixed.astype(jnp.bfloat16)
        conv_float = convolution_output.astype(jnp.float32)
        grouped = convolution_output.reshape(tok_rows, gate_count, block_width)
        results = []
        for scan_direction in range(2):
            gate_matrix_pair = recurrent_gate_blocks[layer_index, scan_direction]
            recurrent_branch = jax.nn.sigmoid(
                jnp.einsum(
                    "tnc,ncd->tnd", grouped, gate_matrix_pair[0], preferred_element_type=jnp.float32
                ).reshape(tok_rows, channels)
            )
            input_gate = jax.nn.sigmoid(
                jnp.einsum(
                    "tnc,ncd->tnd", grouped, gate_matrix_pair[1], preferred_element_type=jnp.float32
                ).reshape(tok_rows, channels)
            )
            decay_logarithm = (
                -RECURRENT_WIDTH
                * jax.nn.softplus(-channel_decay_logit[layer_index, scan_direction])
                * recurrent_branch
                + position_decay_boost[layer_index, scan_direction][:, None]
            )
            is_start = at_first if scan_direction == 0 else at_last
            multiplier = jnp.where(is_start, 1.0, jnp.sqrt(-jnp.expm1(2.0 * decay_logarithm)))
            driven = multiplier * input_gate * conv_float
            results.append(
                lax.associative_scan(
                    combine_pairs,
                    (jnp.exp(decay_logarithm), driven),
                    reverse=scan_direction == 1,
                    axis=0,
                )
            )
        cum_fwd, local_fwd = results[0]
        cum_bwd, local_bwd = results[1]
        all_states = sent_together(
            (cum_fwd[-1:], local_fwd[-1:], cum_bwd[:1], local_bwd[:1]), "sp", 0, 1
        )
        _, incl_fwd = lax.associative_scan(combine_pairs, (all_states[0], all_states[1]), axis=0)
        _, incl_bwd = lax.associative_scan(
            combine_pairs, (all_states[2], all_states[3]), reverse=True, axis=0
        )
        lower_row = lax.dynamic_slice_in_dim(incl_fwd, jnp.maximum(my_index - 1, 0), 1, 0)
        upper_row = lax.dynamic_slice_in_dim(
            incl_bwd, jnp.minimum(my_index + 1, seq_devices - 1), 1, 0
        )
        enter_fwd = jnp.where(my_index > 0, lower_row, 0.0)
        enter_bwd = jnp.where(my_index < seq_devices - 1, upper_row, 0.0)
        state_sum = local_fwd + cum_fwd * enter_fwd + local_bwd + cum_bwd * enter_bwd
        gated = (state_sum * jax.nn.gelu(proj_y.astype(jnp.float32))).astype(jnp.bfloat16)
        partials = jnp.dot(gated, all_out[layer_index], preferred_element_type=jnp.float32).astype(
            jnp.bfloat16
        )
        branch_sum = sum_at_owner(partials.astype(jnp.float32).astype(jnp.bfloat16), "tp", 1)
        stream = (stream.astype(jnp.float32) + branch_sum).astype(jnp.bfloat16)
    return stream


def solution(mesh):
    return jax.shard_map(
        local,
        mesh=mesh,
        in_specs=(
            P(("grp", "sp"), "tp"),
            P(),
            P(None, "sp", "tp"),
            P(None, "sp", "tp"),
            P(None, "tp", "sp"),
            P(None, None, "tp"),
            P(None, None, None, "tp", None, None),
            P(None, None, "tp"),
            P(None, None, ("grp", "sp")),
        ),
        out_specs=P(("grp", "sp"), "tp"),
        check_vma=False,
    )
```

profile of v0, /device:TPU:33, one launch (start us, length us, event | category | flops | bytes accessed | tf_op | source)
XLA Modules:
  0.0 367.1 jit_solution(17647595524314493667)
XLA Ops:
  10.3 5.1 %all-to-all-start = ((bf16[4,256,512]{1,2,0:T(8,128)(2,1)}), bf16[4,256,512]{1,2,0:T(8,128)(2,1)S(1)}, u32[]{:S(2)}, u32[]{:S(2)}) async-start(bf16[4,256,512]{1,2,0:T(8,128)(2,1)} %broadcast_in_dim.58), calls=%async_computation | async-start | bytes 2097152 | tf_op jit(solution)/shard_map/all_to_all | solution.py:18
  16.4 8.8 %all-to-all-done = bf16[4,256,512]{1,2,0:T(8,128)(2,1)S(1)} async-done(((bf16[4,256,512]{1,2,0:T(8,128)(2,1)}), bf16[4,256,512]{1,2,0:T(8,128)(2,1)S(1)}, u32[]{:S(2)}, u32[]{:S(2)}) %all-to-all-start) | async-done | bytes 1048608 | tf_op jit(solution)/shard_map/all_to_all | solution.py:18
  25.8 69.2 %all-gather.6.cloned.1.call-done = bf16[2,2048,384]{2,1,0:T(8,128)(2,1)} async-done(((bf16[2,64,384]{2,1,0:T(8,128)(2,1)}), bf16[2,2048,384]{2,1,0:T(8,128)(2,1)}) %all-gather.6.cloned.1.call-update) | async-done | bytes 3145744 | tf_op jit(solution)/shard_map/all_gather | solution.py:95
  95.0 2.1 fusion.34
  97.2 3.8 %collective-permute-start = (bf16[2,384]{1,0:T(2,128)(2,1)S(1)}, bf16[2,384]{1,0:T(2,128)(2,1)S(1)}, u32[]{:S(2)}, u32[]{:S(2)}) collective-permute-start(bf16[2,384]{1,0:T(2,128)(2,1)S(1)} %get-tuple-element.61), channel_id=1, source_target_pairs={{0,4},{4,8},{8,12},{12,16},{16,20},{20,24},{24,28},{28,32},{32,36}... | collective-permute-start | bytes 4616 | tf_op jit(solution)/shard_map/ppermute | solution.py:35
  101.0 2.0 collective-permute-start.1
  103.0 2.9 collective-permute-done.1
  119.0 29.0 %all-gather = f32[32,1,1536]{2,1,0:T(1,128)S(1)} all-gather(f32[1,1,1536]{2,1,0:T(1,128)S(1)} %maximum_bitcast_fusion), channel_id=1, replica_groups=mesh['grp'=2,'sp'=32,'tp'=4] {'sp'}, dimensions={0}, use_global_device_ids=true | all-gather | bytes 202752 | tf_op jit(solution)/shard_map/all_gather | solution.py:47
  149.5 2.0 rev.12
  151.5 2.0 rev.13
  154.5 10.8 %all-gather.8.cloned.1.call-done = bf16[2,2048,384]{2,1,0:T(8,128)(2,1)} async-done(((bf16[2,64,384]{2,1,0:T(8,128)(2,1)}), bf16[2,2048,384]{2,1,0:T(8,128)(2,1)}) %all-gather.8.cloned.1.call-update) | async-done | bytes 3145744 | tf_op jit(solution)/shard_map/all_gather | solution.py:96
  165.3 70.1 %all-gather.10.cloned.1.call-done = bf16[2,384,2048]{1,2,0:T(8,128)(2,1)} async-done(((bf16[2,384,64]{1,2,0:T(8,128)(2,1)}), bf16[2,384,2048]{1,2,0:T(8,128)(2,1)}) %all-gather.10.cloned.1.call-update) | async-done | bytes 3145744 | tf_op jit(solution)/shard_map/all_gather | solution.py:97
  235.3 3.9 %convolution_convert_fusion.1 = bf16[256,2048]{1,0:T(8,128)(2,1)S(1)} fusion(bf16[2,384,2048]{1,2,0:T(8,128)(2,1)} %all-gather.10.cloned.1.call-done, bf16[256,2048]{0,1:T(8,128)(2,1)S(1)} %bitcast.155, bf16[2,2048,384]{2,1,0:T(8,128)(2,1)} %all-gather.8.cloned.1.call-done, f32[256,384]{1,0:T(8,128)} %rev.13, f32[256,384]{1,0:T(8,128)} %rev.12, ...), kind=kOutput, calls=%fused_computation.5 | convolution fusion | flops 807698432 | bytes 7605248 | tf_op jit(solution)/shard_map/dot_general | solution.py:166
  239.3 18.6 %all_to_all.20 = bf16[4,256,512]{2,1,0:T(8,128)(2,1)S(1)} all-to-all(bf16[4,256,512]{2,1,0:T(8,128)(2,1)S(1)} %bitcast.150), channel_id=1, replica_groups=mesh['grp'=2,'sp'=32,'tp'=4] {'tp'}, dimensions={0} | all-to-all | bytes 2097152 | tf_op jit(solution)/shard_map/all_to_all | solution.py:59
  259.3 3.6 all-to-all-start.2
  262.9 13.7 %all-to-all-done.2 = bf16[4,256,512]{1,2,0:T(8,128)(2,1)S(1)} async-done(((bf16[4,256,512]{1,2,0:T(8,128)(2,1)}), bf16[4,256,512]{1,2,0:T(8,128)(2,1)S(1)}, u32[]{:S(2)}, u32[]{:S(2)}) %all-to-all-start.2) | async-done | bytes 1048608 | tf_op jit(solution)/shard_map/all_to_all | solution.py:18
  279.6 5.4 %collective-permute-start.2 = (bf16[2,384]{1,0:T(2,128)(2,1)S(1)}, bf16[2,384]{1,0:T(2,128)(2,1)S(1)}, u32[]{:S(2)}, u32[]{:S(2)}) collective-permute-start(bf16[2,384]{1,0:T(2,128)(2,1)S(1)} %get-tuple-element.43), channel_id=1, source_target_pairs={{0,4},{4,8},{8,12},{12,16},{16,20},{20,24},{24,28},{28,32},{32,36}... | collective-permute-start | bytes 4616 | tf_op jit(solution)/shard_map/ppermute | solution.py:35
  285.0 2.0 collective-permute-start.3
  287.0 2.9 collective-permute-done.3
  303.1 28.8 %all-gather.1 = f32[32,1,1536]{2,1,0:T(1,128)S(1)} all-gather(f32[1,1,1536]{2,1,0:T(1,128)S(1)} %maximum_bitcast_fusion.1), channel_id=1, replica_groups=mesh['grp'=2,'sp'=32,'tp'=4] {'sp'}, dimensions={0}, use_global_device_ids=true | all-gather | bytes 202752 | tf_op jit(solution)/shard_map/all_gather | solution.py:47
  333.4 2.0 rev.29
  335.4 2.0 rev.30
  338.3 3.9 %convolution_convert_fusion = bf16[256,2048]{1,0:T(8,128)(2,1)S(1)} fusion(bf16[2,384,2048]{1,2,0:T(8,128)(2,1)} %all-gather.10.cloned.1.call-done, bf16[256,2048]{0,1:T(8,128)(2,1)S(1)} %bitcast.157, bf16[2,2048,384]{2,1,0:T(8,128)(2,1)} %all-gather.8.cloned.1.call-done, f32[256,384]{1,0:T(8,128)} %rev.30, f32[256,384]{1,0:T(8,128)} %rev.29, ...), kind=kOutput, calls=%fused_computation.4 | convolution fusion | flops 807698432 | bytes 7605248 | tf_op jit(solution)/shard_map/dot_general | solution.py:166
  342.3 17.3 %all_to_all.21 = bf16[4,256,512]{2,1,0:T(8,128)(2,1)S(1)} all-to-all(bf16[4,256,512]{2,1,0:T(8,128)(2,1)S(1)} %bitcast.151), channel_id=1, replica_groups=mesh['grp'=2,'sp'=32,'tp'=4] {'tp'}, dimensions={0} | all-to-all | bytes 2097152 | tf_op jit(solution)/shard_map/all_to_all | solution.py:59
  (836 shorter events, 37.9 us)
Async XLA Ops:
  6.5 9.6 %copy-start.11 = (f32[2,2048]{1,0:T(2,128)S(1)}, f32[2,2048]{1,0:T(2,128)}, u32[]{:S(2)}) copy-start(f32[2,2048]{1,0:T(2,128)} %param.10) | copy-start | bytes 49156
  6.5 88.5 %all-gather.6.cloned.1.call-start = ((), (), s32[]{:S(2)}) async-start(), calls=%async_computation.4 | async-start | bytes 3244032 | tf_op jit(solution)/shard_map/all_gather | solution.py:95
  7.3 8.9 %copy-start.13 = (f32[2,2,384]{2,1,0:T(2,128)S(1)}, f32[2,2,384]{2,1,0:T(2,128)}, u32[]{:S(2)}) copy-start(f32[2,2,384]{2,1,0:T(2,128)} %param.16) | copy-start | bytes 18436
  7.3 9.0 %copy-start.12 = (f32[2,4,384]{2,1,0:T(4,128)S(1)}, f32[2,4,384]{2,1,0:T(4,128)}, u32[]{:S(2)}) copy-start(f32[2,4,384]{2,1,0:T(4,128)} %param.14) | copy-start | bytes 36868
  7.3 9.0 %copy-start.14 = (f32[2,2,256]{2,1,0:T(2,128)S(1)}, f32[2,2,256]{2,1,0:T(2,128)}, u32[]{:S(2)}) copy-start(f32[2,2,256]{2,1,0:T(2,128)} %param.17) | copy-start | bytes 12292
  7.3 157.9 %all-gather.8.cloned.1.call-start = ((), (), s32[]{:S(2)}) async-start(), calls=%async_computation.5 | async-start | bytes 3244032 | tf_op jit(solution)/shard_map/all_gather | solution.py:96
  10.3 14.9 %all-to-all-start = ((bf16[4,256,512]{1,2,0:T(8,128)(2,1)}), bf16[4,256,512]{1,2,0:T(8,128)(2,1)S(1)}, u32[]{:S(2)}, u32[]{:S(2)}) async-start(bf16[4,256,512]{1,2,0:T(8,128)(2,1)} %broadcast_in_dim.58), calls=%async_computation | async-start | bytes 2097152 | tf_op jit(solution)/shard_map/all_to_all | solution.py:18
  15.4 219.9 %all-gather.10.cloned.1.call-start = ((), (), s32[]{:S(2)}) async-start(), calls=%async_computation.6 | async-start | bytes 3244032 | tf_op jit(solution)/shard_map/all_gather | solution.py:97
  25.8 77.2 %copy-start = (bf16[4,256,512]{1,2,0:T(8,128)(2,1)}, bf16[4,256,512]{1,2,0:T(8,128)(2,1)S(1)}, u32[]{:S(2)}) copy-start(bf16[4,256,512]{1,2,0:T(8,128)(2,1)S(1)} %fusion.2) | copy-start | bytes 3145732
  97.2 9.2 %copy-start.16 = (bf16[2,2,2,3,128,128]{5,4,3,2,1,0:T(8,128)(2,1)S(1)}, bf16[2,2,2,3,128,128]{5,4,3,2,1,0:T(8,128)(2,1)}, u32[]{:S(2)}) copy-start(bf16[2,2,2,3,128,128]{5,4,3,2,1,0:T(8,128)(2,1)} %param.15) | copy-start | bytes 2359300
  97.2 5.8 %collective-permute-start = (bf16[2,384]{1,0:T(2,128)(2,1)S(1)}, bf16[2,384]{1,0:T(2,128)(2,1)S(1)}, u32[]{:S(2)}, u32[]{:S(2)}) collective-permute-start(bf16[2,384]{1,0:T(2,128)(2,1)S(1)} %get-tuple-element.61), channel_id=1, source_target_pairs={{0,4},{4,8},{8,12},{12,16},{16,20},{20,24},{24,28},{28,32},{32,36}... | collective-permute-start | bytes 4616 | tf_op jit(solution)/shard_map/ppermute | solution.py:35
  101.0 4.9 %collective-permute-start.1 = (bf16[2,384]{1,0:T(2,128)(2,1)S(1)}, bf16[2,384]{1,0:T(2,128)(2,1)S(1)}, u32[]{:S(2)}, u32[]{:S(2)}) collective-permute-start(bf16[2,384]{1,0:T(2,128)(2,1)S(1)} %get-tuple-element.62), channel_id=1, source_target_pairs={{4,0},{8,4},{12,8},{16,12},{20,16},{24,20},{28,24},{32,28},{36,32}... | collective-permute-start | bytes 4616 | tf_op jit(solution)/shard_map/ppermute | solution.py:37
  118.9 30.0 %copy-start.8 = (f32[256,384]{1,0:T(8,128)}, f32[256,384]{1,0:T(8,128)S(1)}, u32[]{:S(2)}) copy-start(f32[256,384]{1,0:T(8,128)S(1)} %pad.531) | copy-start | bytes 1179652
  118.9 29.9 %copy-start.10 = (f32[256,384]{1,0:T(8,128)}, f32[256,384]{1,0:T(8,128)S(1)}, u32[]{:S(2)}) copy-start(f32[256,384]{1,0:T(8,128)S(1)} %pad.547) | copy-start | bytes 1179652
  148.9 86.4 %copy-start.1 = (bf16[4,256,512]{1,2,0:T(8,128)(2,1)S(1)}, bf16[4,256,512]{1,2,0:T(8,128)(2,1)}, u32[]{:S(2)}) copy-start(bf16[4,256,512]{1,2,0:T(8,128)(2,1)} %copy-done) | copy-start | bytes 3145732
  239.3 18.7 %copy-start.4 = (bf16[256,512]{1,0:T(8,128)(2,1)S(1)}, bf16[256,512]{1,0:T(8,128)(2,1)}, u32[]{:S(2)}) copy-start(bf16[256,512]{1,0:T(8,128)(2,1)} %param.9) | copy-start | bytes 786436
  259.3 17.3 %all-to-all-start.2 = ((bf16[4,256,512]{1,2,0:T(8,128)(2,1)}), bf16[4,256,512]{1,2,0:T(8,128)(2,1)S(1)}, u32[]{:S(2)}, u32[]{:S(2)}) async-start(bf16[4,256,512]{1,2,0:T(8,128)(2,1)} %broadcast_in_dim.61), calls=%async_computation.2 | async-start | bytes 2097152 | tf_op jit(solution)/shard_map/all_to_all | solution.py:18
  277.3 9.7 %copy-start.2 = (bf16[4,256,512]{1,2,0:T(8,128)(2,1)}, bf16[4,256,512]{1,2,0:T(8,128)(2,1)S(1)}, u32[]{:S(2)}) copy-start(bf16[4,256,512]{1,2,0:T(8,128)(2,1)S(1)} %fusion.5) | copy-start | bytes 3145732
  279.6 10.7 %copy-start.17 = (bf16[2,2,2,3,128,128]{5,4,3,2,1,0:T(8,128)(2,1)S(1)}, bf16[2,2,2,3,128,128]{5,4,3,2,1,0:T(8,128)(2,1)}, u32[]{:S(2)}) copy-start(bf16[2,2,2,3,128,128]{5,4,3,2,1,0:T(8,128)(2,1)} %param.15) | copy-start | bytes 2359300
  279.6 7.4 %collective-permute-start.2 = (bf16[2,384]{1,0:T(2,128)(2,1)S(1)}, bf16[2,384]{1,0:T(2,128)(2,1)S(1)}, u32[]{:S(2)}, u32[]{:S(2)}) collective-permute-start(bf16[2,384]{1,0:T(2,128)(2,1)S(1)} %get-tuple-element.43), channel_id=1, source_target_pairs={{0,4},{4,8},{8,12},{12,16},{16,20},{20,24},{24,28},{28,32},{32,36}... | collective-permute-start | bytes 4616 | tf_op jit(solution)/shard_map/ppermute | solution.py:35
  285.0 4.9 %collective-permute-start.3 = (bf16[2,384]{1,0:T(2,128)(2,1)S(1)}, bf16[2,384]{1,0:T(2,128)(2,1)S(1)}, u32[]{:S(2)}, u32[]{:S(2)}) collective-permute-start(bf16[2,384]{1,0:T(2,128)(2,1)S(1)} %get-tuple-element.44), channel_id=1, source_target_pairs={{4,0},{8,4},{12,8},{16,12},{20,16},{24,20},{28,24},{32,28},{36,32}... | collective-permute-start | bytes 4616 | tf_op jit(solution)/shard_map/ppermute | solution.py:37
  302.9 29.9 %copy-start.5 = (f32[256,384]{1,0:T(8,128)}, f32[256,384]{1,0:T(8,128)S(1)}, u32[]{:S(2)}) copy-start(f32[256,384]{1,0:T(8,128)S(1)} %pad.614) | copy-start | bytes 1179652
  302.9 29.8 %copy-start.7 = (f32[256,384]{1,0:T(8,128)}, f32[256,384]{1,0:T(8,128)S(1)}, u32[]{:S(2)}) copy-start(f32[256,384]{1,0:T(8,128)S(1)} %pad.615) | copy-start | bytes 1179652
  303.0 29.7 %copy-start.9 = (f32[256,384]{1,0:T(8,128)}, f32[256,384]{1,0:T(8,128)S(1)}, u32[]{:S(2)}) copy-start(f32[256,384]{1,0:T(8,128)S(1)} %pad.631) | copy-start | bytes 1179652
  (3 other events, 13.4 us)
Sparse Core Ops, SparseCore 0:
  9.2 85.7 all-gather.5
  96.9 68.3 all-gather.7
  167.2 68.1 all-gather.9
where the time goes:
time: 368 us; the launch traced here: 367 us
  waiting for transfers between devices  181 us (49%)
  blocking collectives  93.7 us (25%)
  local copies, waits for them, and re-layouts  30.1 us (8%)
  starting transfers between devices  21.8 us (6%)
  between operations  17.6 us (5%)
  matrix products  13.1 us (4%)
  other arithmetic  10.2 us (3%)
    all_gather x1, waiting for transfers between devices, local(): lax.all_gather(output_weight, 'sp', axis=2, tiled=True)  70.1 us
    all_gather x1, waiting for transfers between devices, local(): lax.all_gather(convolution_in_weight, 'sp', axis=1, tiled=True)  69.2 us
    all_gather x2, blocking collectives, sent_together(): result = lax.all_gather(both, axis, axis=dim, tiled=True)  57.9 us
    all_to_all x2, blocking collectives, sum_at_owner(): blocks = lax.all_to_all(split_up(array, dim, size), axis, 0, 0, tiled=True)  35.9 us
    all_to_all x2, waiting for transfers between devices, sent_to_all(): lax.all_to_all(jnp.broadcast_to(array[None], (size, *array.shape)), axis,...  22.4 us
    all_gather x1, waiting for transfers between devices, local(): lax.all_gather(gating_in_weight, 'sp', axis=1, tiled=True)  10.8 us
    ppermute x2, starting transfers between devices, extended(): lax.ppermute(tail, axis, [(i, (i + 1) % count) for i in range(ends)])  9.14 us
    all_to_all x2, starting transfers between devices, sent_to_all(): lax.all_to_all(jnp.broadcast_to(array[None], (size, *array.shape)), axis,...  8.72 us
  transfers between devices with their start and end apart: 9, of which 7 were waited for; matrix products, arithmetic and copies ran while one was open for 6% of the time, Pallas kernels for 0%

commit v1 on v0

v1 whole, which is shorter than its diff:
```python
import functools

import jax
import jax.numpy as jnp
from jax import lax
from jax.experimental import pallas as pl
from jax.experimental.pallas import tpu as pltpu
from jax.sharding import PartitionSpec as P

EPS = 1e-06
RECURRENT_WIDTH = 8.0
SEG = 8
LAG = 3
CHUNKS = 2
F32 = jnp.float32
BF16 = jnp.bfloat16
MESH = pl.DeviceIdType.MESH


def dot(a, b):
    return jnp.dot(a, b, preferred_element_type=F32)


def dot_nt(a, b):
    return lax.dot_general(a, b, (((1,), (1,)), ((), ())), preferred_element_type=F32)


def dot_tn(a, b):
    return lax.dot_general(a, b, (((0,), (0,)), ((), ())), preferred_element_type=F32)


def one_minus_square(log_decay, decay):
    u = -2.0 * log_decay
    series = 1.0 - u * (1.0 / 6.0)
    for k in (5.0, 4.0, 3.0, 2.0):
        series = 1.0 - u * (1.0 / k) * series
    return jnp.where(u < 0.25, u * series, 1.0 - decay * decay)


def kernel(
    n_sp,
    n_tp,
    stream,
    gain,
    wx,
    wy,
    wo,
    taps,
    gates,
    logit,
    boost,
    out,
    wfull,
    feat,
    normed,
    px,
    halo_prev,
    halo_next,
    ext,
    conv,
    dec,
    drv,
    gel,
    mine,
    states,
    gated,
    part,
    relay_in,
    rs_left,
    rs_right,
    w_recv,
    w_send,
    pair_recv,
    ag_recv,
    ag_send,
    rs_recv,
    rs_send,
    halo_recv,
    halo_send,
    st_recv,
    st_send,
):
    layers = wx.shape[0]
    rows = stream.shape[0]
    cols = stream.shape[1]
    width = cols * n_tp
    shard = wx.shape[1]
    ch = wx.shape[2]
    block = gates.shape[-1]
    steps = rows // SEG
    mats = 3 * layers
    chips = n_sp // 2
    crow = rows // CHUNKS

    me = lax.axis_index("sp")
    x = lax.axis_index("tp")

    def sp_at(offset):
        return lax.rem(me + (offset + n_sp), n_sp)

    def tp_at(offset):
        return lax.rem(x + (offset + n_tp), n_tp)

    partner = me + 1 - 2 * lax.rem(me, 2)
    xr, xl, xo = tp_at(1), tp_at(-1), tp_at(2)

    def send(src, dst, ssem, rsem, **where):
        pltpu.make_async_remote_copy(
            src_ref=src,
            dst_ref=dst,
            send_sem=ssem,
            recv_sem=rsem,
            device_id=where,
            device_id_type=MESH,
        ).start()

    def landed(ref, sem):
        pltpu.make_async_copy(ref, ref, sem).wait()

    def own_rows(owner):
        return pl.ds(pl.multiple_of(owner * shard, shard), shard)

    def reach(m, d):
        far, near = chips // 2, chips - 1 - chips // 2
        return far if (m + d) % 2 == 0 else near

    def w_slot(m, owner):
        return wfull.at[m, own_rows(owner)]

    def hand_over(m, owner):
        send(w_slot(m, owner), w_slot(m, owner), w_send.at[m], pair_recv.at[m], sp=partner)

    def stage(t):
        for m in range(mats):
            k = t - LAG * m
            if k < 0 or k > chips // 2:
                continue
            for d in range(2):
                if k > reach(m, d):
                    continue
                owner = sp_at(-2 * k if d == 0 else 2 * k)
                if k > 0:
                    landed(w_slot(m, owner), w_hop(m, d, k))
                if k < reach(m, d):
                    send(
                        w_slot(m, owner),
                        w_slot(m, owner),
                        w_send.at[m],
                        w_hop(m, d, k + 1),
                        sp=sp_at(2 if d == 0 else -2),
                    )
                if k > 0 or d == 0:
                    hand_over(m, owner)

    def w_hop(m, d, k):
        return w_recv.at[m, d, k - 1]

    at = [0]
    stages = LAG * (mats - 1) + chips // 2 + 1

    def advance(upto):
        while at[0] <= min(upto, stages - 1):
            stage(at[0])
            at[0] += 1

    def complete(m):
        advance(LAG * m + chips // 2)
        landed(wfull.at[m, pl.ds(0, chips * shard)], pair_recv.at[m])

    def chunk(c):
        return pl.ds(c * crow, crow)

    def gather_send(l, c):
        own = feat.at[l, x, chunk(c)]
        send(own, own, ag_send.at[l], ag_recv.at[l, 0, c], tp=xr)
        send(own, own, ag_send.at[l], ag_recv.at[l, 1, c], tp=xl)

    def gather_relay(l, c):
        from_left = feat.at[l, xl, chunk(c)]
        from_right = feat.at[l, xr, chunk(c)]
        if c % 2 == 0:
            landed(from_left, ag_recv.at[l, 0, c])
            send(from_left, from_left, ag_send.at[l], ag_recv.at[l, 2, c], tp=xr)
            landed(from_right, ag_recv.at[l, 1, c])
        else:
            landed(from_right, ag_recv.at[l, 1, c])
            send(from_right, from_right, ag_send.at[l], ag_recv.at[l, 2, c], tp=xl)
            landed(from_left, ag_recv.at[l, 0, c])

    def gather_end(l, c):
        landed(feat.at[l, xo, chunk(c)], ag_recv.at[l, 2, c])

    barrier = pltpu.get_barrier_semaphore()
    for offset in (1, -1, 2, -2):
        pl.semaphore_signal(barrier, inc=1, device_id={"sp": sp_at(offset)}, device_id_type=MESH)
    for peer in (xr, xl):
        pl.semaphore_signal(barrier, inc=1, device_id={"tp": peer}, device_id_type=MESH)

    row_at = lax.broadcasted_iota(jnp.int32, (rows, rows), 0)
    col_at = lax.broadcasted_iota(jnp.int32, (rows, rows), 1)
    perm = (col_at == lax.rem(row_at, SEG) * steps + row_at // SEG).astype(BF16)
    eye = (
        lax.broadcasted_iota(jnp.int32, (shard, shard), 0)
        == lax.broadcasted_iota(jnp.int32, (shard, shard), 1)
    ).astype(BF16)
    for l in range(layers):
        wfull[3 * l, own_rows(me), :] = wx[l]
        wfull[3 * l + 1, own_rows(me), :] = wy[l]
        wfull[3 * l + 2, own_rows(me), :] = dot_nt(eye, wo[l]).astype(BF16)
    feat[0, x, :, :] = dot(perm, stream[...]).astype(BF16)

    pl.semaphore_wait(barrier, 6)
    advance(0)
    for c in range(CHUNKS):
        gather_send(0, c)

    boost_rows = jnp.concatenate(
        [boost[l, d : d + 1, :] for l in range(layers) for d in range(2)]
        + [jnp.zeros((8 - 2 * layers, rows), F32)],
        axis=0,
    )
    high = boost_rows.astype(BF16)
    rest = boost_rows - high.astype(F32)
    middle = rest.astype(BF16)
    low = (rest - middle.astype(F32)).astype(BF16)
    boost_cols = dot_nt(perm, high) + dot_nt(perm, middle) + dot_nt(perm, low)

    rate = -RECURRENT_WIDTH * jax.nn.softplus(-logit[...])

    advance(1)
    advance(2)
    for c in range(CHUNKS):
        gather_relay(0, c)

    sub = lax.broadcasted_iota(jnp.int32, (SEG, ch), 0)
    row_id = lax.broadcasted_iota(jnp.int32, (rows, 1), 0)

    for l in range(layers):
        if l == 0:
            complete(0)
        for c in range(CHUNKS):
            if l == 0:
                gather_end(l, c)
            total = None
            for o in range(n_tp):
                f = feat[l, o, chunk(c), :].astype(F32)
                s = jnp.sum(f * f, axis=1, keepdims=True)
                total = s if total is None else total + s
            inverse = lax.rsqrt(total * (1.0 / width) + EPS)
            for o in range(n_tp):
                f = feat[l, o, chunk(c), :].astype(F32)
                g = gain[l : l + 1, o * cols : (o + 1) * cols]
                normed[chunk(c), o * cols : (o + 1) * cols] = (f * inverse * g).astype(BF16)
        px_now = dot(normed[...], wfull[3 * l]).astype(BF16)
        px[l] = px_now
        send(px.at[l, pl.ds(0, 16)], halo_next.at[l], halo_send.at[l], halo_recv.at[l, 0], sp=sp_at(-1))
        send(
            px.at[l, pl.ds(rows - 16, 16)], halo_prev.at[l], halo_send.at[l], halo_recv.at[l, 1], sp=sp_at(1)
        )
        if l == 0:
            advance(9)
        else:
            complete(3 * l + 1)
            y = dot(normed[...], wfull[3 * l + 1]).astype(BF16).astype(F32)
            gel[...] = jax.nn.gelu(y)
        ext[SEG : SEG + rows, :] = px_now.astype(F32)
        landed(halo_next.at[l], halo_recv.at[l, 0])
        landed(halo_prev.at[l], halo_recv.at[l, 1])
        before = jnp.where(me > 0, halo_prev[l].astype(F32)[8:16], 0.0)
        after = jnp.where(me < n_sp - 1, halo_next[l].astype(F32), 0.0)
        ext[0:SEG, :] = jnp.where(
            sub == 0, pltpu.roll(before, 1, 0), pltpu.roll(ext[rows : rows + SEG, :], 1, 0)
        )
        for k in range(2):
            ext[SEG + rows + k * SEG : SEG + rows + (k + 1) * SEG, :] = jnp.where(
                sub == SEG - 1,
                pltpu.roll(after[k * SEG : (k + 1) * SEG], SEG - 1, 0),
                pltpu.roll(ext[SEG + k * SEG : SEG + (k + 1) * SEG, :], SEG - 1, 0),
            )
        mixed = taps[l, 0:1, :] * ext[0:rows, :]
        for k in range(1, 4):
            mixed = mixed + taps[l, k : k + 1, :] * ext[k * SEG : k * SEG + rows, :]
        conv[...] = mixed.astype(BF16)
        for b in range(ch // block):
            lanes = slice(b * block, (b + 1) * block)
            cv = conv[:, lanes]
            cvf = cv.astype(F32)
            for d in range(2):
                recur = jax.nn.sigmoid(dot(cv, gates[l, d, 0, b]))
                inject = jax.nn.sigmoid(dot(cv, gates[l, d, 1, b]))
                log_decay = (
                    rate[l, d : d + 1, lanes] * recur + boost_cols[:, 2 * l + d : 2 * l + d + 1]
                )
                decay = jnp.exp(log_decay)
                multiplier = jnp.sqrt(one_minus_square(log_decay, decay))
                if d == 0:
                    first = jnp.logical_and(row_id == 0, me == 0)
                else:
                    first = jnp.logical_and(row_id == rows - 1, me == n_sp - 1)
                multiplier = jnp.where(first, 1.0, multiplier)
                dec[d, :, lanes] = decay
                drv[d, :, lanes] = multiplier * inject * cvf
        if l == 0:
            advance(10)
        carry = [None, None]
        for j in range(steps):
            for d in range(2):
                q = j if d == 0 else steps - 1 - j
                r = slice(q * SEG, (q + 1) * SEG)
                a, h = dec[d, r, :], drv[d, r, :]
                if carry[d] is not None:
                    h = a * carry[d][1] + h
                    a = a * carry[d][0]
                    dec[d, r, :] = a
                    drv[d, r, :] = h
                carry[d] = (a, h)
        into = []
        for d in range(2):
            a, h = carry[d]
            for hop in (1, 2, 4):
                shift = hop if d == 0 else SEG - hop
                inside = sub >= hop if d == 0 else sub < SEG - hop
                a_far, h_far = pltpu.roll(a, shift, 0), pltpu.roll(h, shift, 0)
                h = jnp.where(inside, a * h_far + h, h)
                a = jnp.where(inside, a * a_far, a)
            end = SEG - 1 if d == 0 else 0
            mine[l, d, 0:1, :] = a[end : end + 1, :]
            mine[l, d, 1:2, :] = h[end : end + 1, :]
            shift = 1 if d == 0 else SEG - 1
            inside = sub >= 1 if d == 0 else sub < SEG - 1
            into.append(
                (
                    jnp.where(inside, pltpu.roll(a, shift, 0), 1.0),
                    jnp.where(inside, pltpu.roll(h, shift, 0), 0.0),
                )
            )
        order = sorted(range(1, n_sp), key=lambda o: -min(o, n_sp - o))
        for offset in order:
            wraps = jnp.where(me + offset >= n_sp, 1, 0)
            send(
                mine.at[l, wraps],
                states.at[l, me],
                st_send.at[l],
                st_recv.at[l],
                sp=sp_at(offset),
            )
        states[l, me, :, :] = mine[l, 0]
        if l == 0:
            complete(1)
            y = dot(normed[...], wfull[1]).astype(BF16).astype(F32)
            gel[...] = jax.nn.gelu(y)
            advance(12)
        landed(states.at[l, pl.ds(0, n_sp - 1)], st_recv.at[l])
        enter = []
        for d in range(2):
            e = jnp.zeros((1, ch), F32)
            for q in range(n_sp):
                k = q if d == 0 else n_sp - 1 - q
                take = me > k if d == 0 else me < k
                e = jnp.where(take, states[l, k, 0:1, :] * e + states[l, k, 1:2, :], e)
            enter.append(into[d][0] * e + into[d][1])
        for j in range(steps // 2):
            pieces = []
            for q in (2 * j, 2 * j + 1):
                r = slice(q * SEG, (q + 1) * SEG)
                s = (drv[0, r, :] + dec[0, r, :] * enter[0]) + (drv[1, r, :] + dec[1, r, :] * enter[1])
                pieces.append(s * gel[r, :])
            gated[2 * j * SEG : (2 * j + 2) * SEG, :] = jnp.concatenate(pieces, axis=0).astype(BF16)
        complete(3 * l + 2)

        def partial(dest, c):
            w = wfull[3 * l + 2, pl.ds(pl.multiple_of(dest * cols, cols), cols), :]
            part[l, dest, chunk(c), :] = dot_nt(gated[chunk(c), :], w).astype(BF16)

        def post(dest, c, to, ref, which):
            send(
                part.at[l, dest, chunk(c)],
                ref.at[l, chunk(c)],
                rs_send.at[l],
                rs_recv.at[l, which, c],
                tp=to,
            )

        for c in range(CHUNKS):
            ahead, behind = (xr, xl) if c % 2 == 0 else (xl, xr)
            partial(xo, c)
            post(xo, c, ahead, relay_in, 0)
            partial(behind, c)
            if c % 2 == 0:
                post(behind, c, behind, rs_right, 2)
            else:
                post(behind, c, behind, rs_left, 1)
            partial(ahead, c)
            partial(x, c)
        for c in range(CHUNKS):
            ahead = xr if c % 2 == 0 else xl
            landed(relay_in.at[l, chunk(c)], rs_recv.at[l, 0, c])
            both = part[l, ahead, chunk(c), :].astype(F32) + relay_in[l, chunk(c), :].astype(F32)
            part[l, ahead, chunk(c), :] = both.astype(BF16)
            if c % 2 == 0:
                post(ahead, c, ahead, rs_left, 1)
            else:
                post(ahead, c, ahead, rs_right, 2)
        if l == 0:
            advance(LAG * 3 + chips // 2 - 1)
        for c in range(CHUNKS):
            landed(rs_left.at[l, chunk(c)], rs_recv.at[l, 1, c])
            landed(rs_right.at[l, chunk(c)], rs_recv.at[l, 2, c])
            fresh = (
                feat[l, x, chunk(c), :].astype(F32)
                + part[l, x, chunk(c), :].astype(F32)
                + rs_left[l, chunk(c), :].astype(F32)
                + rs_right[l, chunk(c), :].astype(F32)
            ).astype(BF16)
            if l + 1 < layers:
                feat[l + 1, x, chunk(c), :] = fresh
                gather_send(l + 1, c)
            else:
                normed[chunk(c), 0:cols] = fresh
        if l + 1 < layers:
            for c in range(CHUNKS):
                gather_relay(l + 1, c)
            complete(3 * l + 3)
            for c in range(CHUNKS):
                gather_end(l + 1, c)

    out[...] = dot_tn(perm, normed[:, 0:cols]).astype(BF16)

    for m in range(mats):
        landed(wfull.at[m, pl.ds(0, (2 * chips - 1) * shard)], w_send.at[m])
    for l in range(layers):
        landed(feat.at[l, pl.ds(0, 3)], ag_send.at[l])
        landed(part.at[l, pl.ds(0, 3)], rs_send.at[l])
        landed(px.at[l, pl.ds(0, 32)], halo_send.at[l])
        landed(states.at[l, pl.ds(0, n_sp - 1)], st_send.at[l])


def local(n_sp, n_tp, stream, gain, wx, wy, wo, taps, gates, logit, boost):
    layers, shard, ch = wx.shape
    rows, cols = stream.shape
    width = cols * n_tp
    mats = 3 * layers
    vmem = pl.BlockSpec(memory_space=pltpu.VMEM)
    dma = pltpu.SemaphoreType.DMA
    return pl.pallas_call(
        functools.partial(kernel, n_sp, n_tp),
        out_shape=jax.ShapeDtypeStruct((rows, cols), BF16),
        in_specs=[vmem] * 9,
        out_specs=vmem,
        scratch_shapes=[
            pltpu.VMEM((mats, width, ch), BF16),
            pltpu.VMEM((layers, n_tp, rows, cols), BF16),
            pltpu.VMEM((rows, width), BF16),
            pltpu.VMEM((layers, rows, ch), BF16),
            pltpu.VMEM((layers, 16, ch), BF16),
            pltpu.VMEM((layers, 16, ch), BF16),
            pltpu.VMEM((rows + 3 * SEG, ch), F32),
            pltpu.VMEM((rows, ch), BF16),
            pltpu.VMEM((2, rows, ch), F32),
            pltpu.VMEM((2, rows, ch), F32),
            pltpu.VMEM((rows, ch), F32),
            pltpu.VMEM((layers, 2, 2, ch), F32),
            pltpu.VMEM((layers, n_sp, 2, ch), F32),
            pltpu.VMEM((rows, ch), BF16),
            pltpu.VMEM((layers, n_tp, rows, cols), BF16),
            pltpu.VMEM((layers, rows, cols), BF16),
            pltpu.VMEM((layers, rows, cols), BF16),
            pltpu.VMEM((layers, rows, cols), BF16),
            dma((mats, 2, n_sp // 4)),
            dma((mats,)),
            dma((mats,)),
            dma((layers, 3, CHUNKS)),
            dma((layers,)),
            dma((layers, 3, CHUNKS)),
            dma((layers,)),
            dma((layers, 2)),
            dma((layers,)),
            dma((layers,)),
            dma((layers,)),
        ],
        compiler_params=pltpu.CompilerParams(
            collective_id=0, has_side_effects=True, vmem_limit_bytes=56 * 1024 * 1024
        ),
        name="whole",
    )(stream, gain, wx, wy, wo, taps, gates, logit, boost)


def solution(mesh):
    return jax.shard_map(
        functools.partial(local, mesh.shape["sp"], mesh.shape["tp"]),
        mesh=mesh,
        in_specs=(
            P(("grp", "sp"), "tp"),
            P(),
            P(None, "sp", "tp"),
            P(None, "sp", "tp"),
            P(None, "tp", "sp"),
            P(None, None, "tp"),
            P(None, None, None, "tp", None, None),
            P(None, None, "tp"),
            P(None, None, ("grp", "sp")),
        ),
        out_specs=P(("grp", "sp"), "tp"),
        check_vma=False,
    )
```

time: 368 us -> 149 us (0.40)
  waiting for transfers between devices: 181 us -> 0 us
  Pallas kernels: 0 us -> 145 us
  blocking collectives: 93.7 us -> 0 us
  local copies, waits for them, and re-layouts: 30.1 us -> 3.38 us
  starting transfers between devices: 21.8 us -> 0 us
  between operations: 17.6 us -> 0.01 us
  matrix products: 13.1 us -> 0 us
  other arithmetic: 10.2 us -> 0 us
    all_gather x3 -> x0, waiting for transfers between devices: 150 us -> none  [the longest x1 70.1 us: local(): lax.all_gather(output_weight, 'sp', axis=2, tiled=True)]
    pallas_call x0 -> x1, Pallas kernels: none -> 145 us  [local(): pl.pallas_call(functools.partial(kernel, n_sp, n_tp), out_shape=jax.Shape...]
    all_gather x2 -> x0, blocking collectives: 57.9 us -> none  [sent_together(): result = lax.all_gather(both, axis, axis=dim, tiled=True)]
    all_to_all x2 -> x0, blocking collectives: 35.9 us -> none  [sum_at_owner(): blocks = lax.all_to_all(split_up(array, dim, size), axis, 0, 0, tiled=True)]
    all_to_all x2 -> x0, waiting for transfers between devices: 22.4 us -> none  [sent_to_all(): lax.all_to_all(jnp.broadcast_to(array[None], (size, *array.shape)), axis,...]
    dot_general x12 -> x0, matrix products: 13.1 us -> none  [the longest x2 7.76 us: local(): jnp.dot(gated, all_out[layer_index], preferred_element_type=jnp.float32)]
    ppermute x4 -> x0, starting transfers between devices: 13 us -> none  [the longest x2 9.14 us: extended(): lax.ppermute(tail, axis, [(i, (i + 1) % count) for i in range(ends)])]
    slice x335 -> x0, local copies, waits for them, and re-layouts: 11.1 us -> none  [the longest x220 8.31 us: local(): lax.associative_scan(combine_pairs, (jnp.exp(decay_logarithm), driven), r...]
  transfers between devices with their start and end apart: 9 -> 0, of which waited for: 7 -> 0; matrix products, arithmetic and copies ran while one was open for 6% -> 0% of each run, Pallas kernels for 0% -> 0%
where the time goes in v1:
time: 149 us
  Pallas kernels  145 us (97%)
  local copies, waits for them, and re-layouts  3.38 us (2%)
    pallas_call x1, Pallas kernels, local(): pl.pallas_call(functools.partial(kernel, n_sp, n_tp), out_shape=jax.Shape...  145 us
    unnamed x2, local copies, waits for them, and re-layouts  3.38 us

profile of v1, /device:TPU:33, one launch (start us, length us, event | category | flops | bytes accessed | tf_op | source)
XLA Modules:
  0.0 148.9 jit_solution(5494654821093609014)
XLA Ops:
  0.0 1.7 %copy.10.wo = bf16[2,384,64]{2,1,0:T(8,128)(2,1)} copy(bf16[2,384,64]{1,2,0:T(8,128)(2,1)} %param.13) | data formatting | bytes 196608 | tf_op args[4]
  1.7 145.5 %whole.1 = bf16[256,512]{1,0:T(8,128)(2,1)} custom-call(bf16[256,512]{1,0:T(8,128)(2,1)} %stream.1, f32[2,2048]{1,0:T(2,128)} %gain.1, bf16[2,64,384]{2,1,0:T(8,128)(2,1)} %wx.1, bf16[2,64,384]{2,1,0:T(8,128)(2,1)} %wy.1, bf16[2,384,64]{2,1,0:T(8,128)(2,1)} %copy.10.wo, f32[2,4,384]{2,1,0:T(4,128)} %taps.1, bf16[2,2,2,3,128,128]{5,4,3,2,1,0:T(8,128)(2,1)} %gates.1, ...), custom_call_target="tpu_custom_call" | custom-call | tf_op jit(solution)/shard_map/whole/pallas_call | solution.py:445
  147.2 1.7 %copy.12 = bf16[256,512]{1,0:T(8,128)(2,1)} copy(bf16[256,512]{1,0:T(8,128)(2,1)} %whole.1) | data formatting | bytes 524288
